TPU v7x, 32 devices: a whole 2x2x4 slice. The times are simulated.
32 devices in a mesh: grp: 2 (over y), sp: 4 (over z), tp: 4 (over x, core).
Axes of the slice: x: 2, y: 2, z: 4, core: 2. Of those that a mesh axis runs over, the one named last changes fastest.
Arguments:
- residual_in: bfloat16 [2048, 2048], P(('grp', 'sp', 'tp')), parts along dimension 0, may hold values from -6 to 6
- q_small: bfloat16 [2048, 1024], P(('grp', 'sp'), 'tp'), parts along dimension 0, may hold values from -5 to 5
- k_small: bfloat16 [2048, 256], P(('grp', 'sp'), 'tp'), parts along dimension 0, may hold values from -5 to 5
- v_small: bfloat16 [2048, 256], P(('grp', 'sp'), 'tp'), parts along dimension 0, may hold values from -6 to 6
- q_large: bfloat16 [2048, 1024], P(('grp', 'sp'), 'tp'), parts along dimension 0, may hold values from -5 to 5
- k_large: bfloat16 [2048, 512], P(('grp', 'sp'), 'tp'), parts along dimension 0, may hold values from -5 to 5
- v_large: bfloat16 [2048, 512], P(('grp', 'sp'), 'tp'), parts along dimension 0, may hold values from -6 to 6
- gain_qs: float32 [64], replicated, may hold values from 0.24 to 7.4
- gain_ks: float32 [64], replicated, may hold values from 0.24 to 7.4
- gain_ql: float32 [128], replicated, may hold values from 0.24 to 7.4
- gain_kl: float32 [128], replicated, may hold values from 0.24 to 7.4
- w_out_small: bfloat16 [1024, 2048], P('tp'), may hold values from -0.125 to 0.125
- w_out_large: bfloat16 [1024, 2048], P('tp'), may hold values from -0.125 to 0.125
- g_ffn: float32 [2048], replicated, may hold values from 0.1 to 1.9
- routes: int32 [2048, 4], P(('grp', 'sp', 'tp')), parts along dimension 0, may hold values from 0 to 7, all different within a row; in each aligned block of 64 rows (0 to 63, 64 to 127, ...) at most 64 rows name the same one
- route_w: float32 [2048, 4], P(('grp', 'sp', 'tp')), parts along dimension 0, may hold values from 0.2 to 1
- w_gate: bfloat16 [8, 2048, 1024], P('sp', None, 'tp'), may hold values from -0.125 to 0.125
- w_up: bfloat16 [8, 2048, 1024], P('sp', None, 'tp'), may hold values from -0.125 to 0.125
- w_down: bfloat16 [8, 1024, 2048], P('sp', 'tp'), may hold values from -0.1875 to 0.1875
- ws_gate: bfloat16 [2048, 1024], P(None, 'tp'), may hold values from -0.125 to 0.125
- ws_up: bfloat16 [2048, 1024], P(None, 'tp'), may hold values from -0.125 to 0.125
- ws_down: bfloat16 [1024, 2048], P('tp'), may hold values from -0.1875 to 0.1875
Outputs:
- result: bfloat16 [2048, 2048], P(('grp', 'sp', 'tp')), parts along dimension 0
There are 2 independent parts, one for each index of `grp`. A program takes and returns all parts, laid end to end along the dimension named above; an argument that names none is the same for every part. Nothing has to cross between parts.
Inputs may be any that keep to these rules, and one draw needn't show every extreme that they name: `routes`: each row names 4 different experts. Among the rows of one device no expert is named more than 64 times, a bound that some block reaches.
All inputs are finite; a program needn't handle non-finite values.
Results may differ from a plain program's by a relative error of at most 0.018.
The roundings to bfloat16 on the way count: a program that leaves them out, or rounds other values in their place, can miss the bound.
Values may be sent and summed in bfloat16 or wider, within the bound.
A program may use at most 128 MiB of HBM per device.

v0:
```python
import math

import jax
import jax.numpy as jnp
from jax import lax
from jax.sharding import PartitionSpec as P

GRID_W = 64
TOPK = 4


norm_eps = 1e-06
rope_base = 10000.0
far_below = -1e30


def rotate_pairs(values, angles):
    front_half, back_half = jnp.split(values, 2, axis=-1)
    cosine_vals = jnp.cos(angles)[:, None, :]
    sine_vals = jnp.sin(angles)[:, None, :]
    return jnp.concatenate(
        [
            front_half * cosine_vals - back_half * sine_vals,
            front_half * sine_vals + back_half * cosine_vals,
        ],
        axis=-1,
    )


def norm_rotate(heads_in, gain, positions, grid_width):
    channels = gain.shape[0]
    values = heads_in.astype(jnp.float32).reshape(heads_in.shape[0], -1, channels)
    values = values * lax.rsqrt(jnp.mean(values * values, axis=-1, keepdims=True) + norm_eps) * gain
    quarter = channels // 4
    inverse = 1.0 / rope_base ** (jnp.arange(quarter, dtype=jnp.float32) / quarter)
    grid_rows = (positions // grid_width).astype(jnp.float32)
    grid_cols = (positions % grid_width).astype(jnp.float32)
    half_width = channels // 2
    turned = jnp.concatenate(
        [
            rotate_pairs(values[..., :half_width], grid_rows[:, None] * inverse[None, :]),
            rotate_pairs(values[..., half_width:], grid_cols[:, None] * inverse[None, :]),
        ],
        axis=-1,
    )
    return turned.astype(jnp.bfloat16)


def absorb(carried, segment, queries):
    peak_val, totals, mixture = carried
    kv_heads = queries.shape[1]
    channels = queries.shape[3]
    pairs = segment.reshape(segment.shape[0], 2, kv_heads, channels)
    scores = jnp.einsum(
        "qkgd,skd->kgqs", queries, pairs[:, 0], preferred_element_type=jnp.float32
    ) * channels ** (-0.5)
    new_peak = jnp.maximum(peak_val, jnp.max(scores, axis=-1))
    weights_raw = jnp.exp(scores - new_peak[..., None])
    shrink = jnp.exp(peak_val - new_peak)
    totals = totals * shrink + jnp.sum(weights_raw, axis=-1)
    update = jnp.einsum(
        "kgqs,skd->qkgd",
        weights_raw.astype(jnp.bfloat16),
        pairs[:, 1],
        preferred_element_type=jnp.float32,
    )
    mixture = mixture * jnp.transpose(shrink, (2, 0, 1))[..., None] + update
    return (new_peak, totals, mixture)


def absorb_blocks(carried, segment, queries):
    row_count = segment.shape[0]
    block_rows = math.gcd(row_count, 1024)
    stacked = segment.reshape(row_count // block_rows, block_rows, segment.shape[1])

    def fold_step(inner, key_block):
        return (absorb(inner, key_block, queries), None)

    carried, _ = lax.scan(fold_step, carried, stacked)
    return carried


def start_state(queries):
    local_rows, kv_heads, group, channels = queries.shape
    return (
        jnp.full((kv_heads, group, local_rows), far_below, jnp.float32),
        jnp.zeros((kv_heads, group, local_rows), jnp.float32),
        jnp.zeros(queries.shape, jnp.float32),
    )


def finish(carried):
    peak_val, totals, mixture = carried
    heads_out = mixture / jnp.transpose(totals, (2, 0, 1))[..., None]
    return heads_out.reshape(heads_out.shape[0], -1).astype(jnp.bfloat16)


def local(
    residual_in,
    q_small,
    k_small,
    v_small,
    q_large,
    k_large,
    v_large,
    gain_qs,
    gain_ks,
    gain_ql,
    gain_kl,
    w_out_small,
    w_out_large,
    g_ffn,
    routes,
    route_w,
    w_gate,
    w_up,
    w_down,
    ws_gate,
    ws_up,
    ws_down,
):
    local_rows = q_small.shape[0]
    positions = lax.axis_index("sp") * local_rows + jnp.arange(local_rows, dtype=jnp.int32)
    query_small = norm_rotate(q_small, gain_qs, positions, GRID_W)
    key_small = norm_rotate(k_small, gain_ks, positions, GRID_W)
    query_large = norm_rotate(q_large, gain_ql, positions, GRID_W)
    key_large = norm_rotate(k_large, gain_kl, positions, GRID_W)
    query_small = query_small.reshape(local_rows, key_small.shape[1], -1, gain_qs.shape[0])
    query_large = query_large.reshape(local_rows, key_large.shape[1], -1, gain_ql.shape[0])
    pack_small = jnp.concatenate([key_small.reshape(local_rows, -1), v_small], axis=1)
    pack_large = jnp.concatenate([key_large.reshape(local_rows, -1), v_large], axis=1)
    segment = (
        lax.all_gather(pack_small, "sp", axis=0, tiled=True),
        lax.all_gather(pack_large, "sp", axis=0, tiled=True),
    )
    heads_small = finish(absorb_blocks(start_state(query_small), segment[0], query_small))
    heads_large = finish(absorb_blocks(start_state(query_large), segment[1], query_large))
    tp_count = lax.axis_size("tp")
    sp_count = lax.axis_size("sp")
    rows_dev = local_rows // tp_count
    head_sum = lax.psum_scatter(
        (
            jnp.dot(heads_small, w_out_small, preferred_element_type=jnp.float32)
            + jnp.dot(heads_large, w_out_large, preferred_element_type=jnp.float32)
        ).astype(jnp.bfloat16),
        "tp",
        scatter_dimension=0,
        tiled=True,
    ).astype(jnp.float32)
    stream = (residual_in.astype(jnp.float32) + head_sum).astype(jnp.bfloat16)
    stream32 = lax.optimization_barrier(stream).astype(jnp.float32)
    normed = (
        stream32
        * lax.rsqrt(jnp.mean(stream32 * stream32, axis=-1, keepdims=True) + norm_eps)
        * g_ffn
    ).astype(jnp.bfloat16)
    channels = normed.shape[1]
    segment = lax.all_gather(normed, "tp", axis=0, tiled=True)
    gate_act = jnp.dot(segment, ws_gate, preferred_element_type=jnp.float32)
    up_act = jnp.dot(segment, ws_up, preferred_element_type=jnp.float32)
    hidden_shared = (jax.nn.silu(gate_act) * up_act).astype(jnp.bfloat16)
    shared = lax.psum_scatter(
        jnp.dot(hidden_shared, ws_down, preferred_element_type=jnp.float32).astype(jnp.bfloat16),
        "tp",
        scatter_dimension=0,
        tiled=True,
    ).astype(jnp.float32)
    local_experts = w_gate.shape[0]
    experts = local_experts * sp_count
    capacity = max(2, 2 * rows_dev * TOPK // experts)
    flat_ids = routes.reshape(-1)
    one_hot = (flat_ids[:, None] == jnp.arange(experts, dtype=jnp.int32)[None, :]).astype(jnp.int32)
    slot_ids = jnp.sum((jnp.cumsum(one_hot, axis=0) - 1) * one_hot, axis=1)
    targets = flat_ids * capacity + slot_ids
    owners = jnp.arange(rows_dev * TOPK, dtype=jnp.int32) // TOPK
    outbox = jnp.zeros((experts * capacity, channels), jnp.bfloat16).at[targets].set(normed[owners])
    arrived = lax.all_to_all(outbox, "sp", split_axis=0, concat_axis=0, tiled=True)
    arrived = lax.all_gather(
        arrived.reshape(sp_count, 1, local_experts, capacity, channels), "tp", axis=1, tiled=True
    )
    gate_act = jnp.einsum("abecd,edf->abecf", arrived, w_gate, preferred_element_type=jnp.float32)
    up_act = jnp.einsum("abecd,edf->abecf", arrived, w_up, preferred_element_type=jnp.float32)
    hidden = (jax.nn.silu(gate_act) * up_act).astype(jnp.bfloat16)
    partial_value = jnp.einsum(
        "abecf,efd->abecd", hidden, w_down, preferred_element_type=jnp.float32
    )
    summed = lax.psum_scatter(
        partial_value.astype(jnp.bfloat16), "tp", scatter_dimension=1, tiled=True
    )
    returned = lax.all_to_all(
        summed.reshape(sp_count * local_experts * capacity, channels),
        "sp",
        split_axis=0,
        concat_axis=0,
        tiled=True,
    )
    picked = returned[targets].reshape(rows_dev, TOPK, channels).astype(jnp.float32)
    routed = jnp.sum(picked * route_w[..., None], axis=1)
    return (stream32 + routed + shared).astype(jnp.bfloat16)


def solution(mesh):
    placed = (
        P(("grp", "sp", "tp"), None),
        P(("grp", "sp"), "tp"),
        P(("grp", "sp"), "tp"),
        P(("grp", "sp"), "tp"),
        P(("grp", "sp"), "tp"),
        P(("grp", "sp"), "tp"),
        P(("grp", "sp"), "tp"),
        P(),
        P(),
        P(),
        P(),
        P("tp", None),
        P("tp", None),
        P(),
        P(("grp", "sp", "tp"), None),
        P(("grp", "sp", "tp"), None),
        P("sp", None, "tp"),
        P("sp", None, "tp"),
        P("sp", "tp", None),
        P(None, "tp"),
        P(None, "tp"),
        P("tp", None),
    )
    return jax.shard_map(
        local, mesh=mesh, in_specs=placed, out_specs=P(("grp", "sp", "tp"), None), check_vma=False
    )
```

profile of v0, /device:TPU:0, one launch (start us, length us, event | category | flops | bytes accessed | tf_op | source)
XLA Modules:
  0.0 444.8 jit_solution(15207383969475351975)
XLA Ops:
  6.6 1.1 copy.48
  7.9 0.9 copy.45
  8.9 0.7 fusion.57
  9.7 1.0 multiply_cosine_fusion.1
  10.8 0.2 constant_dynamic-update-slice_fusion.8
  11.0 0.2 constant_dynamic-update-slice_fusion.7
  11.2 0.2 constant_dynamic-update-slice_fusion.6
  11.6 17.4 %all_gather.13 = bf16[1024,256]{0,1:T(8,128)(2,1)S(1)} all-gather(bf16[256,256]{0,1:T(8,128)(2,1)S(1)} %constant_dynamic-update-slice_fusion.5), channel_id=1, replica_groups=mesh['grp'=2,'sp'=4,'tp'=4] {'sp'}, dimensions={0}, use_global_device_ids=true | all-gather | bytes 655360 | tf_op jit(solution)/shard_map/all_gather | solution.py:134
  29.0 0.8 multiply_multiply_fusion
  29.8 0.3 subtract_convert_fusion.1
  30.0 0.6 bitcast_reduce_fusion.1
  30.7 1.3 copy-done.2
  32.0 0.4 fusion.19
  33.5 14.7 %all_gather.12 = bf16[1024,128]{0,1:T(8,128)(2,1)S(1)} all-gather(bf16[256,128]{0,1:T(8,128)(2,1)S(1)} %constant_dynamic-update-slice_fusion), channel_id=1, replica_groups=mesh['grp'=2,'sp'=4,'tp'=4] {'sp'}, dimensions={0}, use_global_device_ids=true | all-gather | bytes 327680 | tf_op jit(solution)/shard_map/all_gather | solution.py:133
  48.3 0.7 bitcast_reduce_fusion
  49.1 0.7 fusion.1
  49.8 0.8 fusion.32
  50.7 0.4 copy-done.4
  51.1 0.5 fusion.123
  51.5 0.8 copy-done.3
  52.4 0.5 fusion.36
  52.9 1.5 fusion.3
  54.4 0.2 all-gather.3.cloned.1.call-start
  54.9 0.6 reduce-window.6
  55.5 0.2 slice_reduce_fusion
  56.1 24.2 %reduce-scatter.6.cloned.1.call-done = bf16[64,2048]{1,0:T(8,128)(2,1)} async-done(((bf16[256,2048]{1,0:T(8,128)(2,1)}), bf16[64,2048]{1,0:T(8,128)(2,1)}) %reduce-scatter.6.cloned.1.call-update) | async-done | bytes 262160 | tf_op jit(solution)/shard_map/reduce_scatter | solution.py:141
  80.4 1.0 add_convert_fusion
  81.7 7.1 %scatter_custom_fusion = bf16[512,2048]{1,0:T(8,128)(2,1)} fusion(s32[256]{0:T(256)S(1)} %bitcast.254, bf16[64,2048]{1,0:T(8,128)(2,1)S(1)} %fusion.46, s32[1024]{0:T(1024)S(1)} %pad_clamp_fusion.1, bf16[]{:T(256)} %constant.140.clone.1), kind=kCustom, calls=%fused_computation.43 | custom fusion | bytes 2097154 | tf_op jit(solution)/shard_map/scatter | solution.py:176
  88.8 52.6 %all_to_all.21 = bf16[4,128,2048]{2,1,0:T(8,128)(2,1)S(1)} all-to-all(bf16[4,128,2048]{2,1,0:T(8,128)(2,1)} %bitcast.245), channel_id=1, replica_groups=mesh['grp'=2,'sp'=4,'tp'=4] {'sp'}, dimensions={0} | all-to-all | bytes 4194304 | tf_op jit(solution)/shard_map/all_to_all | solution.py:177
  141.4 1.5 copy.55
  142.9 0.3 all-reduce.3.cloned.1.call-start
  143.2 56.3 %all-gather.3.cloned.1.call-done = bf16[4,4,2,64,2048]{4,3,1,0,2:T(8,128)(2,1)} async-done(((bf16[4,1,2,64,2048]{4,3,1,0,2:T(8,128)(2,1)}), bf16[4,4,2,64,2048]{4,3,1,0,2:T(8,128)(2,1)}) %all-gather.3.cloned.1.call-update) | async-done | bytes 8388624 | tf_op jit(solution)/shard_map/all_gather | solution.py:178
  199.4 7.7 %fusion.6 = f32[2,4,4,64,256]{4,3,2,1,0:T(8,128)} fusion(bf16[4,4,2,64,2048]{4,3,1,0,2:T(8,128)(2,1)} %all-gather.3.cloned.1.call-done, bf16[2,2048,256]{2,1,0:T(8,128)(2,1)} %param.39), kind=kOutput, calls=%fused_computation.14 | convolution fusion | flops 2147483648 | bytes 12582912 | tf_op jit(solution)/shard_map/abecd,edf->abecf/dot_general | solution.py:182
  207.1 13.5 %convert_bitcast_fusion = bf16[4,4,2,64,2048]{4,3,1,0,2:T(8,128)(2,1)} fusion(bf16[2,256,2048]{2,1,0:T(8,128)(2,1)S(1)} %copy-done, f32[2,4,4,64,256]{4,3,2,1,0:T(8,128)} %fusion.6, bf16[4,4,2,64,2048]{4,3,1,0,2:T(8,128)(2,1)} %all-gather.3.cloned.1.call-done, bf16[2,2048,256]{2,1,0:T(8,128)(2,1)} %param.38), kind=kOutput, calls=%fused_computation.3 | convolution fusion | flops 4302307328 | bytes 23068672 | tf_op jit(solution)/shard_map/abecf,efd->abecd/dot_general | solution.py:184
  220.7 0.5 all-gather.5.cloned.1.call-update
  221.3 0.6 dynamic-slice.2
  221.9 151.8 %all-reduce.3.cloned.1.call-done = bf16[4,4,2,64,2048]{4,3,1,0,2:T(8,128)(2,1)} async-done(((bf16[4,4,2,64,2048]{4,3,1,0,2:T(8,128)(2,1)}), bf16[4,4,2,64,2048]{4,3,1,0,2:T(8,128)(2,1)}) %all-reduce.3.cloned.1.call-update) | async-done | bytes 8388624
  373.7 2.4 constant_dynamic-slice_fusion
  376.1 1.6 copy.56
  377.7 4.7 %all-to-all-start.1 = ((bf16[4,128,2048]{2,1,0:T(8,128)(2,1)}), bf16[4,128,2048]{2,1,0:T(8,128)(2,1)S(1)}, u32[]{:S(2)}, u32[]{:S(2)}) async-start(bf16[4,128,2048]{2,1,0:T(8,128)(2,1)} %bitcast.244), calls=%async_computation.2 | async-start | bytes 4194304 | tf_op jit(solution)/shard_map/all_to_all | solution.py:190
  382.4 9.5 %all-gather.5.cloned.1.call-done = bf16[256,2048]{1,0:T(8,128)(2,1)} async-done(((bf16[64,2048]{1,0:T(8,128)(2,1)}), bf16[256,2048]{1,0:T(8,128)(2,1)}) %all-gather.5.cloned.1.call-update) | async-done | bytes 1048592 | tf_op jit(solution)/shard_map/all_gather | solution.py:158
  392.0 2.4 fusion.124
  394.3 4.2 convolution_convert_fusion
  398.7 31.6 %all-to-all-done.1 = bf16[4,128,2048]{2,1,0:T(8,128)(2,1)S(1)} async-done(((bf16[4,128,2048]{2,1,0:T(8,128)(2,1)}), bf16[4,128,2048]{2,1,0:T(8,128)(2,1)S(1)}, u32[]{:S(2)}, u32[]{:S(2)}) %all-to-all-start.1) | async-done | bytes 2097184 | tf_op jit(solution)/shard_map/all_to_all | solution.py:190
  430.3 1.4 gather_fusion
  431.7 1.7 reshape.862
  433.4 3.2 multiply_reduce_fusion
  436.6 1.7 fusion.48
  (90 shorter events, 3.1 us)
Async XLA Ops:
  6.5 200.6 %copy-start = (bf16[2,256,2048]{2,1,0:T(8,128)(2,1)S(1)}, bf16[2,256,2048]{2,1,0:T(8,128)(2,1)}, u32[]{:S(2)}) copy-start(bf16[2,256,2048]{2,1,0:T(8,128)(2,1)} %param.40) | copy-start | bytes 6291460
  6.5 4.9 %copy-start.11 = (bf16[256,128]{1,0:T(8,128)(2,1)S(1)}, bf16[256,128]{1,0:T(8,128)(2,1)}, u32[]{:S(2)}) copy-start(bf16[256,128]{1,0:T(8,128)(2,1)} %param.28) | copy-start | bytes 196612
  6.5 73.8 %reduce-scatter.6.cloned.1.call-start = ((), (), s32[]{:S(2)}) async-start(), calls=%async_computation.4 | async-start | bytes 1310720 | tf_op jit(solution)/shard_map/reduce_scatter | solution.py:141
  30.0 2.6 copy-start.9
  30.7 1.4 copy-start.2
  30.7 2.1 copy-start.10
  30.7 2.1 copy-start.16
  30.7 2.8 copy-start.12
  30.7 17.5 %copy-start.17 = (f32[64]{0:T(128)S(1)}, f32[64]{0:T(128)}, u32[]{:S(2)}) copy-start(f32[64]{0:T(128)} %param.29) | copy-start | bytes 772
  49.8 1.2 copy-start.4
  50.7 1.7 copy-start.3
  51.5 1.4 copy-start.7
  52.9 1.7 copy-start.14
  52.9 27.5 %copy-start.8 = (bf16[64,2048]{1,0:T(8,128)(2,1)S(1)}, bf16[64,2048]{1,0:T(8,128)(2,1)}, u32[]{:S(2)}) copy-start(bf16[64,2048]{1,0:T(8,128)(2,1)} %param.22) | copy-start | bytes 786436
  54.4 27.2 %copy-start.13 = (f32[2048]{0:T(1024)S(1)}, f32[2048]{0:T(1024)}, u32[]{:S(2)}) copy-start(f32[2048]{0:T(1024)} %param.35) | copy-start | bytes 24580
  54.4 145.1 %all-gather.3.cloned.1.call-start = ((), (), s32[]{:S(2)}) async-start(), calls=%async_computation.5 | async-start | bytes 10485760 | tf_op jit(solution)/shard_map/all_gather | solution.py:178
  81.7 59.7 %copy-start.5 = (bf16[64,2048]{1,0:T(8,128)(2,1)}, bf16[64,2048]{1,0:T(8,128)(2,1)S(1)}, u32[]{:S(2)}) copy-start(bf16[64,2048]{1,0:T(8,128)(2,1)S(1)} %fusion.46) | copy-start | bytes 786436
  142.9 230.8 %all-reduce.3.cloned.1.call-start = ((), (), s32[]{:S(2)}) async-start(), calls=%async_computation.8 | async-start | bytes 16777216
  220.6 0.7 copy-start.18
  220.6 171.3 %all-gather.5.cloned.1.call-start = ((), (), s32[]{:S(2)}) async-start(), calls=%async_computation.6 | async-start | bytes 1310720 | tf_op jit(solution)/shard_map/all_gather | solution.py:158
  377.7 14.3 %copy-start.6 = (bf16[2048,256]{1,0:T(8,128)(2,1)S(1)}, bf16[2048,256]{1,0:T(8,128)(2,1)}, u32[]{:S(2)}) copy-start(bf16[2048,256]{1,0:T(8,128)(2,1)} %param.41) | copy-start | bytes 3145732
  377.7 52.6 %all-to-all-start.1 = ((bf16[4,128,2048]{2,1,0:T(8,128)(2,1)}), bf16[4,128,2048]{2,1,0:T(8,128)(2,1)S(1)}, u32[]{:S(2)}, u32[]{:S(2)}) async-start(bf16[4,128,2048]{2,1,0:T(8,128)(2,1)} %bitcast.244), calls=%async_computation.2 | async-start | bytes 4194304 | tf_op jit(solution)/shard_map/all_to_all | solution.py:190
  382.4 54.2 %reduce-scatter.8.cloned.1.call-start = ((), (), s32[]{:S(2)}) async-start(), calls=%async_computation.7 | async-start | bytes 1310720 | tf_op jit(solution)/shard_map/reduce_scatter | solution.py:162
  394.3 4.2 copy-start.15
  431.6 6.7 %copy-start.1 = (bf16[2,256,2048]{2,1,0:T(8,128)(2,1)S(1)}, bf16[2,256,2048]{2,1,0:T(8,128)(2,1)}, u32[]{:S(2)}) copy-start(bf16[2,256,2048]{2,1,0:T(8,128)(2,1)} %param.40) | copy-start | bytes 6291460
Sparse Core Ops, SparseCore 0:
  54.5 25.8 reduce-scatter.5
  143.0 56.3 all-gather.2
  220.8 152.8 all-reduce.2
  375.1 16.8 all-gather.4
  398.7 24.7 reduce-scatter.7
where the time goes:
time: 445 us
  waiting for transfers between devices  274 us (62%)
  blocking collectives  84.7 us (19%)
  matrix products  32.4 us (7%)
  local copies, waits for them, and re-layouts  22.1 us (5%)
  between operations  13.6 us (3%)
  other arithmetic  12.8 us (3%)
  starting transfers between devices  5.26 us (1%)
    unnamed x6, waiting for transfers between devices  152 us
    all_gather x1, waiting for transfers between devices, local(): lax.all_gather(arrived.reshape(sp_count, 1, local_experts, capacity, chan...  56.3 us
    all_to_all x1, blocking collectives, local(): lax.all_to_all(outbox, 'sp', split_axis=0, concat_axis=0, tiled=True)  52.6 us
    all_to_all x1, waiting for transfers between devices, local(): lax.all_to_all(summed.reshape(sp_count * local_experts * capacity, channe...  31.6 us
    reduce_scatter x1, waiting for transfers between devices, local(): lax.psum_scatter((jnp.dot(heads_small, w_out_small, preferred_element_typ...  24.2 us
    all_gather x1, blocking collectives, local(): lax.all_gather(pack_large, 'sp', axis=0, tiled=True)  17.4 us
    all_gather x1, blocking collectives, local(): lax.all_gather(pack_small, 'sp', axis=0, tiled=True)  14.7 us
    dot_general x1, matrix products, local(): jnp.einsum('abecf,efd->abecd', hidden, w_down, preferred_element_type=jnp...  13.5 us
  transfers between devices with their start and end apart: 6, of which 5 were waited for; matrix products, arithmetic and copies ran while one was open for 4% of the time, Pallas kernels for 0%

commit v1 on v0

--- a/solution.py
+++ b/solution.py
@@ -1,8 +1,11 @@
+import functools
 import math
 
 import jax
 import jax.numpy as jnp
 from jax import lax
+from jax.experimental import pallas as pl
+from jax.experimental.pallas import tpu as pltpu
 from jax.sharding import PartitionSpec as P
 
 GRID_W = 64
@@ -199,6 +202,323 @@
     return (stream32 + routed + shared).astype(jnp.bfloat16)
 
 
+MESH = pl.DeviceIdType.MESH
+
+
+def greet(peers):
+    barrier = pltpu.get_barrier_semaphore()
+    for peer in peers:
+        pl.semaphore_signal(barrier, inc=1, device_id=peer, device_id_type=MESH)
+    pl.semaphore_wait(barrier, len(peers))
+
+
+def remote(src, dst, send, recv, peer):
+    return pltpu.make_async_remote_copy(
+        src_ref=src, dst_ref=dst, send_sem=send, recv_sem=recv, device_id=peer, device_id_type=MESH
+    )
+
+
+def gather_kernel(n, pack_ref, out_ref, send, recv):
+    me = lax.axis_index("sp")
+    peers = [{"sp": lax.rem(me + k, n)} for k in range(1, n)]
+    greet(peers)
+    copies = [
+        remote(pack_ref, out_ref.at[me], send.at[k], recv.at[k], peer)
+        for k, peer in enumerate(peers)
+    ]
+    for copy in copies:
+        copy.start()
+    out_ref[me] = pack_ref[...]
+    for copy in copies:
+        copy.wait()
+
+
+def gather_rows(pack):
+    n = lax.axis_size("sp")
+    rows, width = pack.shape
+    gathered = pl.pallas_call(
+        functools.partial(gather_kernel, n),
+        out_shape=jax.ShapeDtypeStruct((n, rows, width), pack.dtype),
+        in_specs=[pl.BlockSpec(memory_space=pltpu.VMEM)],
+        out_specs=pl.BlockSpec(memory_space=pltpu.VMEM),
+        scratch_shapes=[pltpu.SemaphoreType.DMA((n - 1,)), pltpu.SemaphoreType.DMA((n - 1,))],
+        compiler_params=pltpu.CompilerParams(collective_id=1, has_side_effects=True),
+    )(pack)
+    return gathered.reshape(n * rows, width)
+
+
+def f32dot(a, b):
+    return jnp.dot(a, b, preferred_element_type=jnp.float32)
+
+
+def layer_kernel(
+    n_sp, n_local, resid, hs, hl, gain, wts, wos, wol, wg_h, wu_h, wd_h, sg_h, su_h, sd_h,
+    out_ref,
+    wg, wu, wd, sg, su, sd, part, pc, psx, px, blk, stream, gath, acc, ybuf, rc, sx, rx, sz, rz, own,
+    wsem, psend, precv, zsend, xsend, csend, grecv, ycs, ycr, yxs, yxr, yzs, yzr,
+):
+    s = lax.axis_index("sp")
+    t = lax.axis_index("tp")
+    rows, width = resid.shape
+    xp = lax.rem(t + 2, 4)
+    cp = t + 1 - 2 * lax.rem(t, 2)
+    cxp = lax.rem(cp + 2, 4)
+    peers = [{"sp": lax.rem(s + k, n_sp)} for k in range(1, n_sp)] + [{"tp": xp}, {"tp": cp}]
+    loads = [
+        pltpu.make_async_copy(src, dst, wsem.at[i])
+        for i, (src, dst) in enumerate(
+            ((sg_h, sg), (su_h, su), (sd_h, sd), (wg_h, wg), (wu_h, wu), (wd_h, wd))
+        )
+    ]
+    greet(peers)
+    for load in loads:
+        load.start()
+
+    def strip(index):
+        return pl.ds(pl.multiple_of(index * rows, rows), rows)
+
+    part[...] = (f32dot(hs[...], wos[...]) + f32dot(hl[...], wol[...])).astype(jnp.bfloat16)
+    to_x = remote(part.at[strip(cxp)], pc.at[1], psend.at[0], precv.at[0], {"tp": cp})
+    to_own = remote(part.at[strip(cp)], pc.at[0], psend.at[1], precv.at[1], {"tp": cp})
+    to_x.start()
+    to_own.start()
+    to_x.wait_recv()
+    psx[...] = (part[strip(xp)].astype(jnp.float32) + pc[1].astype(jnp.float32)).astype(jnp.bfloat16)
+    across = remote(psx, px, psend.at[2], precv.at[2], {"tp": xp})
+    across.start()
+    to_own.wait_recv()
+    across.wait_recv()
+    head_sum = part[strip(t)].astype(jnp.float32) + pc[0].astype(jnp.float32) + px[...].astype(jnp.float32)
+    summed = (resid[...].astype(jnp.float32) + head_sum).astype(jnp.bfloat16)
+    stream[...] = summed
+    wide = summed.astype(jnp.float32)
+    scale = lax.rsqrt(jnp.mean(wide * wide, axis=-1, keepdims=True) + norm_eps)
+    blk[:, :width] = (wide * scale * gain[...]).astype(jnp.bfloat16)
+    blk[:, width:] = wts[...]
+
+    mine = gath.at[s, strip(t)]
+    z_out = [
+        remote(blk, mine, zsend.at[k], grecv.at[s, t], {"sp": lax.rem(s + k + 1, n_sp)})
+        for k in range(n_sp - 1)
+    ]
+    x_own = remote(blk, mine, xsend.at[0], grecv.at[s, t], {"tp": xp})
+    c_own = remote(blk, mine, csend.at[0, 0], grecv.at[s, t], {"tp": cp})
+    x_own.start()
+    for copy in z_out:
+        copy.start()
+    c_own.start()
+    gath[s, strip(t)] = blk[...]
+    for load in loads:
+        load.wait()
+
+    def block_of(k, column):
+        row = lax.rem(s - k + n_sp, n_sp)
+        return gath.at[row, strip(column)], grecv.at[row, column]
+
+    def pass_on(k, column, send, peer):
+        ref, sem = block_of(k, column)
+        return remote(ref, ref, send, sem, peer)
+
+    def core_part(k, slot):
+        index = cp if slot == 0 else cxp
+        return remote(ybuf.at[k, strip(index)], rc.at[k, slot], ycs.at[k, slot], ycr.at[k, slot], {"tp": cp})
+
+    def x_part(k):
+        return remote(sx.at[k], rx.at[k], yxs.at[k], yxr.at[k], {"tp": xp})
+
+    def z_part(k):
+        return remote(sz.at[k], rz.at[k], yzs.at[k], yzr.at[k], {"sp": lax.rem(s - k + n_sp, n_sp)})
+
+    @pl.loop(0, n_sp + 2)
+    def _(k):
+        @pl.when(k < n_sp - 1)
+        def _():
+            ahead = pass_on(k + 1, t, xsend.at[k + 1], {"tp": xp})
+            ahead.wait_recv()
+            ahead.start()
+            pass_on(k + 1, t, csend.at[k + 1, 0], {"tp": cp}).start()
+
+        @pl.when(k < n_sp)
+        def _():
+            over = pass_on(k, xp, csend.at[k, 1], {"tp": cp})
+            over.wait_recv()
+            over.start()
+            pass_on(k, cp, csend.at[k, 0], {"tp": cp}).wait_recv()
+            pass_on(k, cxp, csend.at[k, 1], {"tp": cp}).wait_recv()
+            row = lax.rem(s - k + n_sp, n_sp)
+            tokens = gath[row, :, :width]
+            marks = gath[row, :, width:].astype(jnp.float32)
+            lane = lax.broadcasted_iota(jnp.int32, marks.shape, 1)
+
+            @pl.when(k == 0)
+            def _():
+                gate = f32dot(tokens, sg[...])
+                hidden = (gate / (1.0 + jnp.exp(-gate)) * f32dot(tokens, su[...])).astype(jnp.bfloat16)
+                acc[...] = f32dot(hidden, sd[...])
+
+            @pl.when(k > 0)
+            def _():
+                acc[...] = jnp.zeros_like(acc)
+
+            experts = n_local * n_sp
+            for e in range(n_local):
+                number = s * n_local + e
+                hit = (lane == number) | (lane == number + experts) | (lane == number + 2 * experts)
+                weight = jnp.sum(jnp.where(hit, marks, 0.0), axis=1, keepdims=True)
+                gate = f32dot(tokens, wg[e])
+                hidden = (gate / (1.0 + jnp.exp(-gate)) * f32dot(tokens, wu[e])).astype(jnp.bfloat16)
+                acc[...] += weight * f32dot(hidden, wd[e])
+            ybuf[k] = acc[...].astype(jnp.bfloat16)
+            core_part(k, 1).start()
+            core_part(k, 0).start()
+
+        @pl.when((k >= 1) & (k <= n_sp))
+        def _():
+            j = k - 1
+            core_part(j, 1).wait_recv()
+            sx[j] = (ybuf[j, strip(xp)].astype(jnp.float32) + rc[j, 1].astype(jnp.float32)).astype(jnp.bfloat16)
+            x_part(j).start()
+
+        @pl.when(k >= 2)
+        def _():
+            j = k - 2
+            core_part(j, 0).wait_recv()
+            x_part(j).wait_recv()
+            total = ybuf[j, strip(t)].astype(jnp.float32) + rc[j, 0].astype(jnp.float32) + rx[j].astype(jnp.float32)
+
+            @pl.when(j > 0)
+            def _():
+                sz[j] = total.astype(jnp.bfloat16)
+                z_part(j).start()
+
+            @pl.when(j == 0)
+            def _():
+                own[...] = total
+
+    result = stream[...].astype(jnp.float32) + own[...]
+    for k in range(1, n_sp):
+        z_part(k).wait_recv()
+        result = result + rz[k].astype(jnp.float32)
+    out_ref[...] = result.astype(jnp.bfloat16)
+
+    to_x.wait_send()
+    to_own.wait_send()
+    across.wait_send()
+    x_own.wait_send()
+    c_own.wait_send()
+    for copy in z_out:
+        copy.wait_send()
+    for k in range(n_sp):
+        if k > 0:
+            pass_on(k, t, xsend.at[k], {"tp": xp}).wait_send()
+            pass_on(k, t, csend.at[k, 0], {"tp": cp}).wait_send()
+            z_part(k).wait_send()
+        pass_on(k, xp, csend.at[k, 1], {"tp": cp}).wait_send()
+        core_part(k, 0).wait_send()
+        core_part(k, 1).wait_send()
+        x_part(k).wait_send()
+
+
+def layer_call(resid, hs, hl, gain, wts, wos, wol, wg, wu, wd, sg, su, sd):
+    n_sp = lax.axis_size("sp")
+    n_tp = lax.axis_size("tp")
+    rows, width = resid.shape
+    n_local = wg.shape[0]
+    padded = width + wts.shape[1]
+    bf, f32 = jnp.bfloat16, jnp.float32
+    dma = pltpu.SemaphoreType.DMA
+    vmem = pl.BlockSpec(memory_space=pltpu.VMEM)
+    anywhere = pl.BlockSpec(memory_space=pl.ANY)
+    scratch = [pltpu.VMEM(w.shape, w.dtype) for w in (wg, wu, wd, sg, su, sd)] + [
+        pltpu.VMEM((n_tp * rows, width), bf),
+        pltpu.VMEM((2, rows, width), bf),
+        pltpu.VMEM((rows, width), bf),
+        pltpu.VMEM((rows, width), bf),
+        pltpu.VMEM((rows, padded), bf),
+        pltpu.VMEM((rows, width), bf),
+        pltpu.VMEM((n_sp, n_tp * rows, padded), bf),
+        pltpu.VMEM((n_tp * rows, width), f32),
+        pltpu.VMEM((n_sp, n_tp * rows, width), bf),
+        pltpu.VMEM((n_sp, 2, rows, width), bf),
+        pltpu.VMEM((n_sp, rows, width), bf),
+        pltpu.VMEM((n_sp, rows, width), bf),
+        pltpu.VMEM((n_sp, rows, width), bf),
+        pltpu.VMEM((n_sp, rows, width), bf),
+        pltpu.VMEM((rows, width), f32),
+        dma((6,)), dma((3,)), dma((3,)),
+        dma((n_sp - 1,)), dma((n_sp,)), dma((n_sp, 2)), dma((n_sp, n_tp)),
+        dma((n_sp, 2)), dma((n_sp, 2)), dma((n_sp,)), dma((n_sp,)), dma((n_sp,)), dma((n_sp,)),
+    ]
+    return pl.pallas_call(
+        functools.partial(layer_kernel, n_sp, n_local),
+        out_shape=jax.ShapeDtypeStruct((rows, width), bf),
+        in_specs=[vmem] * 7 + [anywhere] * 6,
+        out_specs=vmem,
+        scratch_shapes=scratch,
+        compiler_params=pltpu.CompilerParams(
+            collective_id=2, has_side_effects=True, vmem_limit_bytes=48 * 1024 * 1024
+        ),
+    )(resid, hs, hl, gain, wts, wos, wol, wg, wu, wd, sg, su, sd)
+
+
+def attend(queries, keys, values):
+    rows, heads, group, channels = queries.shape
+    keys = keys.reshape(keys.shape[0], heads, channels)
+    values = values.reshape(values.shape[0], heads, channels)
+    scores = jnp.einsum("qkgd,skd->kgqs", queries, keys, preferred_element_type=jnp.float32) * channels ** (-0.5)
+    raised = jnp.exp(scores - jnp.max(scores, axis=-1, keepdims=True))
+    totals = jnp.sum(raised, axis=-1)
+    mixture = jnp.einsum(
+        "kgqs,skd->qkgd", raised.astype(jnp.bfloat16), values, preferred_element_type=jnp.float32
+    )
+    mixture = mixture / jnp.transpose(totals, (2, 0, 1))[..., None]
+    return mixture.reshape(rows, -1).astype(jnp.bfloat16)
+
+
+def dense_local(
+    residual_in, q_small, k_small, v_small, q_large, k_large, v_large,
+    gain_qs, gain_ks, gain_ql, gain_kl, w_out_small, w_out_large, g_ffn,
+    routes, route_w, w_gate, w_up, w_down, ws_gate, ws_up, ws_down,
+):
+    local_rows = q_small.shape[0]
+    positions = lax.axis_index("sp") * local_rows + jnp.arange(local_rows, dtype=jnp.int32)
+    key_small = norm_rotate(k_small, gain_ks, positions, GRID_W)
+    key_large = norm_rotate(k_large, gain_kl, positions, GRID_W)
+    kv_small, kv_large = key_small.shape[1], key_large.shape[1]
+    pack = jnp.concatenate(
+        [key_small.reshape(local_rows, -1), v_small, key_large.reshape(local_rows, -1), v_large], axis=1
+    )
+    gathered = gather_rows(pack)
+    query_small = norm_rotate(q_small, gain_qs, positions, GRID_W)
+    query_large = norm_rotate(q_large, gain_ql, positions, GRID_W)
+    query_small = query_small.reshape(local_rows, kv_small, -1, gain_qs.shape[0])
+    query_large = query_large.reshape(local_rows, kv_large, -1, gain_ql.shape[0])
+    a, b = k_small.shape[1], k_large.shape[1]
+    heads_small = attend(query_small, gathered[:, :a], gathered[:, a : 2 * a])
+    heads_large = attend(query_large, gathered[:, 2 * a : 2 * a + b], gathered[:, 2 * a + b :])
+    experts = w_gate.shape[0] * lax.axis_size("sp")
+    named = routes[:, :, None] == jnp.arange(experts, dtype=jnp.int32)
+    marks = jnp.sum(jnp.where(named, route_w[:, :, None], 0.0), axis=1)
+    first = lax.reduce_precision(marks, 8, 7)
+    second = lax.reduce_precision(marks - first, 8, 7)
+    third = marks - first - second
+    marks = jnp.concatenate([first, second, third], axis=1)
+    marks = jnp.pad(marks, ((0, 0), (0, 128 - marks.shape[1]))).astype(jnp.bfloat16)
+    return layer_call(
+        residual_in, heads_small, heads_large, g_ffn[None, :], marks, w_out_small, w_out_large,
+        w_gate, w_up, w_down, ws_gate, ws_up, ws_down,
+    )
+
+
+def fits_dense(mesh, *arrays):
+    routes, w_gate = arrays[14], arrays[16]
+    ways = mesh.shape["sp"] * mesh.shape["tp"]
+    rows_dev = routes.shape[0] // (ways * mesh.shape["grp"])
+    experts = w_gate.shape[0]
+    capacity = max(2, 2 * rows_dev * TOPK // experts)
+    return mesh.shape["tp"] == 4 and capacity >= rows_dev and 3 * experts <= 128
+
+
 def solution(mesh):
     placed = (
         P(("grp", "sp", "tp"), None),
@@ -224,6 +544,11 @@
         P(None, "tp"),
         P("tp", None),
     )
-    return jax.shard_map(
-        local, mesh=mesh, in_specs=placed, out_specs=P(("grp", "sp", "tp"), None), check_vma=False
-    )
+
+    def whole(*arrays):
+        body = dense_local if fits_dense(mesh, *arrays) else local
+        return jax.shard_map(
+            body, mesh=mesh, in_specs=placed, out_specs=P(("grp", "sp", "tp"), None), check_vma=False
+        )(*arrays)
+
+    return whole

time: 445 us -> 128 us (0.29)
  waiting for transfers between devices: 274 us -> 0 us
  Pallas kernels: 0 us -> 108 us
  blocking collectives: 84.7 us -> 0 us
  matrix products: 32.4 us -> 4.79 us
  local copies, waits for them, and re-layouts: 22.1 us -> 8.04 us
  between operations: 13.6 us -> 0.38 us
  other arithmetic: 12.8 us -> 7.11 us
  starting transfers between devices: 5.26 us -> 0 us
    unnamed x6 -> x0, waiting for transfers between devices: 152 us -> none
    pallas_call x0 -> x2, Pallas kernels: none -> 108 us  [the longest x1 87.1 us: layer_call(): pl.pallas_call(functools.partial(layer_kernel, n_sp, n_local), out_shape=...]
    all_gather x2 -> x0, waiting for transfers between devices: 65.8 us -> none  [the longest x1 56.3 us: local(): lax.all_gather(arrived.reshape(sp_count, 1, local_experts, capacity, chan...]
    all_to_all x1 -> x0, blocking collectives: 52.6 us -> none  [local(): lax.all_to_all(outbox, 'sp', split_axis=0, concat_axis=0, tiled=True)]
    all_gather x2 -> x0, blocking collectives: 32.1 us -> none  [the longest x1 17.4 us: local(): lax.all_gather(pack_large, 'sp', axis=0, tiled=True)]
    all_to_all x1 -> x0, waiting for transfers between devices: 31.6 us -> none  [local(): lax.all_to_all(summed.reshape(sp_count * local_experts * capacity, channe...]
    dot_general x10 -> x4, matrix products: 32.4 us -> 4.79 us  [the longest x2 2.55 us: attend(): jnp.einsum('kgqs,skd->qkgd', raised.astype(jnp.bfloat16), values, preferr...]
    reduce_scatter x2 -> x0, waiting for transfers between devices: 24.2 us -> none  [the longest x1 24.2 us: local(): lax.psum_scatter((jnp.dot(heads_small, w_out_small, preferred_element_typ...]
  transfers between devices with their start and end apart: 6 -> 0, of which waited for: 5 -> 0; matrix products, arithmetic and copies ran while one was open for 4% -> 0% of each run, Pallas kernels for 0% -> 0%
where the time goes in v1:
time: 128 us
  Pallas kernels  108 us (84%)
  local copies, waits for them, and re-layouts  8.04 us (6%)
  other arithmetic  7.11 us (6%)
  matrix products  4.79 us (4%)
    pallas_call x1, Pallas kernels, layer_call(): pl.pallas_call(functools.partial(layer_kernel, n_sp, n_local), out_shape=...  87.1 us
    pallas_call x1, Pallas kernels, gather_rows(): pl.pallas_call(functools.partial(gather_kernel, n), out_shape=jax.ShapeDt...  20.6 us
    unnamed x36, local copies, waits for them, and re-layouts  5.67 us

profile of v1, /device:TPU:0, one launch (start us, length us, event | category | flops | bytes accessed | tf_op | source)
XLA Modules:
  0.0 128.0 jit_solution(7943091678204219198)
XLA Ops:
  0.0 1.0 copy.85
  1.1 0.7 multiply_multiply_fusion.1
  1.9 0.2 multiply_cosine_fusion.7
  2.1 0.9 copy.77
  3.0 0.1 fusion.42
  3.1 0.8 fusion.44
  3.9 1.2 fusion.80
  5.1 0.0 copy-done.11
  5.1 0.1 copy.82
  5.3 0.0 copy-done.8
  5.3 0.1 fusion.45
  5.4 0.0 copy-done.14
  5.4 0.1 fusion.47
  5.5 1.2 fusion.84
  6.7 0.0 copy-done.10
  6.8 0.9 concatenate.54.pack_ref
  7.7 20.6 %shard_map.208 = bf16[4,256,384]{2,1,0:T(8,128)(2,1)} custom-call(bf16[256,384]{1,0:T(8,128)(2,1)} %concatenate.54.pack_ref), custom_call_target="tpu_custom_call" | custom-call | tf_op jit(solution)/shard_map/pallas_call | solution.py:239
  28.3 1.6 %bitcast_reduce_fusion = (f32[4,256]{1,0:T(4,128)S(1)}, f32[1024,256,4]{1,0,2:T(8,128)S(1)}) fusion(bf16[256,4,16]{0,2,1:T(8,128)(2,1)S(1)} %get-tuple-element.15, bf16[256,4,16]{0,2,1:T(8,128)(2,1)S(1)} %get-tuple-element.16, bf16[256,4,16]{0,2,1:T(8,128)(2,1)S(1)} %get-tuple-element.10, bf16[256,4,16]{0,2,1:T(8,128)(2,1)S(1)} %get-tuple-element.9, ...), kind=kOutput, calls=%fused_computation.1 | convolution fusion | flops 136838144 | bytes 4591616 | tf_op jit(solution)/shard_map/qkgd,skd->kgqs/dot_general | solution.py:468
  29.9 0.0 copy-start.7
  29.9 0.7 fusion.1
  30.6 0.4 copy-done.7
  31.1 0.9 fusion.17
  32.0 0.1 copy.93.hs
  32.1 0.0 copy-done.9
  32.1 0.1 copy.87
  32.2 0.1 copy.88
  32.4 0.0 copy-done.15
  32.4 0.1 multiply_multiply_fusion
  32.5 1.0 multiply_cosine_fusion.1
  33.5 0.3 subtract_convert_fusion.1
  33.8 0.6 bitcast_reduce_fusion.1
  34.4 0.0 copy-start.12
  34.4 0.0 copy-start.13
  34.4 0.4 fusion.7
  34.8 0.0 copy-start
  34.8 0.0 copy-start.1
  34.8 0.0 copy-start.2
  34.8 0.0 copy-start.6
  34.8 1.6 %fusion.13 = bf16[256,1,2,128]{0,3,2,1:T(8,128)(2,1)S(1)} fusion(f32[1024,256,2]{1,0,2:T(8,128)S(1)} %get-tuple-element.47, f32[2,256]{1,0:T(2,128)S(1)} %get-tuple-element.46, bf16[1024,384]{1,0:T(8,128)(2,1)} %bitcast.122, f32[256,2]{0,1:T(2,128)S(1)} %bitcast.129), kind=kOutput, calls=%fused_computation.15 | convolution fusion | flops 135921664 | bytes 2494464 | tf_op jit(solution)/shard_map/kgqs,skd->qkgd/dot_general | solution.py:471
  36.5 0.1 copy.98.hl
  36.6 0.0 copy-done.12
  36.6 0.1 copy.92
  36.8 0.0 copy-start.3
  36.8 1.2 copy-done.3
  38.0 1.2 copy-done.4
  39.2 0.9 copy-done.5
  40.2 87.1 %shard_map.209 = bf16[64,2048]{1,0:T(8,128)(2,1)S(1)} custom-call(bf16[64,2048]{1,0:T(8,128)(2,1)S(1)} %copy-done.5, bf16[256,256]{1,0:T(8,128)(2,1)S(1)} %copy.93.hs, bf16[256,256]{1,0:T(8,128)(2,1)S(1)} %copy.98.hl, f32[1,2048]{1,0:T(1,128)S(1)} %bitcast.120, bf16[64,128]{1,0:T(8,128)(2,1)S(1)} %pad.5.wts, bf16[256,2048]{1,0:T(8,128)(2,1)S(1)} %copy-done, ...), custom_call_target="tpu_custom_call" | custom-call | tf_op jit(solution)/shard_map/pallas_call | solution.py:452
  127.2 0.7 copy.102
  (27 shorter events, 0.2 us)
Async XLA Ops:
  0.0 5.1 %copy-start.11 = (bf16[256,64]{0,1:T(8,128)(2,1)S(1)}, bf16[256,64]{0,1:T(8,128)(2,1)}, u32[]{:S(2)}) copy-start(bf16[256,64]{0,1:T(8,128)(2,1)} %param.25) | copy-start | bytes 98308
  0.0 5.3 %copy-start.8 = (bf16[256,128]{1,0:T(8,128)(2,1)S(1)}, bf16[256,128]{1,0:T(8,128)(2,1)}, u32[]{:S(2)}) copy-start(bf16[256,128]{1,0:T(8,128)(2,1)} %param.27) | copy-start | bytes 196612
  0.0 5.4 %copy-start.14 = (f32[128]{0:T(128)S(1)}, f32[128]{0:T(128)}, u32[]{:S(2)}) copy-start(f32[128]{0:T(128)} %param.32) | copy-start | bytes 1540
  0.0 6.7 %copy-start.10 = (bf16[256,128]{1,0:T(8,128)(2,1)S(1)}, bf16[256,128]{1,0:T(8,128)(2,1)}, u32[]{:S(2)}) copy-start(bf16[256,128]{1,0:T(8,128)(2,1)} %param.28) | copy-start | bytes 196612
  29.9 1.1 copy-start.7
  31.0 1.0 copy-start.9
  31.1 1.3 %copy-start.15 = (f32[128]{0:T(128)S(1)}, f32[128]{0:T(128)}, u32[]{:S(2)}) copy-start(f32[128]{0:T(128)} %param.31) | copy-start | bytes 1540
  34.4 2.2 %copy-start.12 = (f32[64,4]{0,1:T(4,128)S(1)}, f32[64,4]{0,1:T(4,128)}, u32[]{:S(2)}) copy-start(f32[64,4]{0,1:T(4,128)} %param.37) | copy-start | bytes 3076
  34.4 2.2 %copy-start.13 = (s32[64,4]{0,1:T(4,128)S(1)}, s32[64,4]{0,1:T(4,128)}, u32[]{:S(2)}) copy-start(s32[64,4]{0,1:T(4,128)} %param.36) | copy-start | bytes 3076
  34.8 2.0 %copy-start = (bf16[256,2048]{1,0:T(8,128)(2,1)S(1)}, bf16[256,2048]{1,0:T(8,128)(2,1)}, u32[]{:S(2)}) copy-start(bf16[256,2048]{1,0:T(8,128)(2,1)} %wos.1) | copy-start | bytes 3145732
  34.8 2.0 %copy-start.1 = (bf16[256,2048]{1,0:T(8,128)(2,1)S(1)}, bf16[256,2048]{1,0:T(8,128)(2,1)}, u32[]{:S(2)}) copy-start(bf16[256,2048]{1,0:T(8,128)(2,1)} %wol.1) | copy-start | bytes 3145732
  34.8 2.0 %copy-start.2 = (bf16[2048,256]{1,0:T(8,128)(2,1)S(1)}, bf16[2048,256]{1,0:T(8,128)(2,1)}, u32[]{:S(2)}) copy-start(bf16[2048,256]{1,0:T(8,128)(2,1)} %sg_h.1) | copy-start | bytes 3145732
  34.8 2.0 %copy-start.6 = (f32[2048]{0:T(1024)S(1)}, f32[2048]{0:T(1024)}, u32[]{:S(2)}) copy-start(f32[2048]{0:T(1024)} %param.35) | copy-start | bytes 24580
  36.8 1.2 copy-start.3
  38.0 1.2 copy-start.4
  39.2 0.9 copy-start.5

commit v2 on v1

--- a/solution.py
+++ b/solution.py
@@ -218,44 +218,137 @@
     )
 
 
-def gather_kernel(n, pack_ref, out_ref, send, recv):
-    me = lax.axis_index("sp")
-    peers = [{"sp": lax.rem(me + k, n)} for k in range(1, n)]
-    greet(peers)
-    copies = [
-        remote(pack_ref, out_ref.at[me], send.at[k], recv.at[k], peer)
-        for k, peer in enumerate(peers)
-    ]
-    for copy in copies:
-        copy.start()
-    out_ref[me] = pack_ref[...]
-    for copy in copies:
-        copy.wait()
-
-
-def gather_rows(pack):
-    n = lax.axis_size("sp")
-    rows, width = pack.shape
-    gathered = pl.pallas_call(
-        functools.partial(gather_kernel, n),
-        out_shape=jax.ShapeDtypeStruct((n, rows, width), pack.dtype),
-        in_specs=[pl.BlockSpec(memory_space=pltpu.VMEM)],
-        out_specs=pl.BlockSpec(memory_space=pltpu.VMEM),
-        scratch_shapes=[pltpu.SemaphoreType.DMA((n - 1,)), pltpu.SemaphoreType.DMA((n - 1,))],
-        compiler_params=pltpu.CompilerParams(collective_id=1, has_side_effects=True),
-    )(pack)
-    return gathered.reshape(n * rows, width)
-
-
 def f32dot(a, b):
     return jnp.dot(a, b, preferred_element_type=jnp.float32)
 
 
+def rotated(tile, turn_c, turn_s, channels):
+    lanes = tile.shape[1]
+    row = lax.broadcasted_iota(jnp.int32, (lanes, lanes), 0)
+    column = lax.broadcasted_iota(jnp.int32, (lanes, lanes), 1)
+    swap = jnp.where((row ^ column) == channels // 4, 1.0, 0.0).astype(jnp.bfloat16)
+    same = jnp.where((row ^ column) < channels, 1.0, 0.0).astype(jnp.bfloat16)
+    wide = tile.astype(jnp.float32)
+    square = wide * wide
+    upper = square.astype(jnp.bfloat16)
+    lower = (square - upper.astype(jnp.float32)).astype(jnp.bfloat16)
+    mean = (f32dot(upper, same) + f32dot(lower, same)) * (1.0 / channels)
+    return lax.rsqrt(mean + norm_eps) * (wide * turn_c + f32dot(tile, swap) * turn_s)
+
+
+def attention(
+    s, n_sp, small, large, heads_in, v_large, turn_c, turn_s,
+    kv_own, kv, q_s, q_l, p_s, p_l, hs, hl, kvr, kup, kdown,
+):
+    rows = heads_in.shape[0]
+    n_small, n_large = q_s.shape[0] // rows, q_l.shape[0] // rows
+
+    def turned(start, channels):
+        lanes = pl.ds(start, 128)
+        return rotated(heads_in[:, lanes], turn_c[:, lanes], turn_s[:, lanes], channels)
+
+    first = n_small * small
+    mixed = turned(first, small)
+    lane = lax.broadcasted_iota(jnp.int32, mixed.shape, 1)
+    plain = heads_in[:, pl.ds(first, 128)].astype(jnp.float32)
+    kv_own[:, 0:128] = jnp.where(lane < small, mixed, plain).astype(jnp.bfloat16)
+    kv_own[:, 128:256] = turned(first + 128 + n_large * large, large).astype(jnp.bfloat16)
+    kv_own[:, 256:384] = v_large[...]
+
+    def send(source, row, sems, step, target):
+        return pltpu.make_async_remote_copy(
+            src_ref=source, dst_ref=kv.at[row], send_sem=sems.at[step], recv_sem=kvr.at[row],
+            device_id={"sp": lax.rem(target + n_sp, n_sp)}, device_id_type=MESH,
+        )
+
+    @pl.when(s < n_sp - 1)
+    def _():
+        send(kv_own, s, kup, 0, s + 1).start()
+
+    @pl.when(s > 0)
+    def _():
+        send(kv_own, s, kdown, 0, s - 1).start()
+
+    kv[s] = kv_own[...]
+    for tile in range(n_small * small // 128):
+        both = turned(tile * 128, small).astype(jnp.bfloat16)
+        for half in range(128 // small):
+            q_s[pl.ds((tile * (128 // small) + half) * rows, rows), :] = both[:, half * small : (half + 1) * small]
+    for tile in range(n_large):
+        q_l[pl.ds(tile * rows, rows), :] = turned(first + 128 + tile * 128, large).astype(jnp.bfloat16)
+
+    def score(row):
+        span = pl.ds(pl.multiple_of(row * rows, rows), rows)
+        keys = kv[row, :, 0:small]
+        p_s[:, span] = lax.dot_general(
+            q_s[...], keys, (((1,), (1,)), ((), ())), preferred_element_type=jnp.float32
+        ) * small ** (-0.5)
+        keys = kv[row, :, 128:256]
+        p_l[:, span] = lax.dot_general(
+            q_l[...], keys, (((1,), (1,)), ((), ())), preferred_element_type=jnp.float32
+        ) * large ** (-0.5)
+
+    score(s)
+
+    @pl.loop(1, n_sp)
+    def _(d):
+        below, above = s - d, s + d
+
+        @pl.when(below >= 0)
+        def _():
+            send(kv.at[below], below, kup, d, s + 1).wait_recv()
+
+            @pl.when(s < n_sp - 1)
+            def _():
+                send(kv.at[below], below, kup, d, s + 1).start()
+
+        @pl.when(above < n_sp)
+        def _():
+            send(kv.at[above], above, kdown, d, s - 1).wait_recv()
+
+            @pl.when(s > 0)
+            def _():
+                send(kv.at[above], above, kdown, d, s - 1).start()
+
+        @pl.when(below >= 0)
+        def _():
+            score(below)
+
+        @pl.when(above < n_sp)
+        def _():
+            score(above)
+
+    def head(index, scores, low, width, out):
+        block = scores[pl.ds(index * rows, rows), :]
+        raised = jnp.exp(block - jnp.max(block, axis=-1, keepdims=True))
+        total = jnp.sum(raised, axis=-1, keepdims=True)
+        weights = raised.astype(jnp.bfloat16)
+        mixture = f32dot(weights[:, :rows], kv[0, :, low : low + width])
+        for row in range(1, n_sp):
+            mixture += f32dot(weights[:, row * rows : (row + 1) * rows], kv[row, :, low : low + width])
+        out[:, index * width : (index + 1) * width] = (mixture / total).astype(jnp.bfloat16)
+
+    for index in range(n_small):
+        head(index, p_s, small, small, hs)
+    for index in range(n_large):
+        head(index, p_l, 256, large, hl)
+
+    @pl.loop(0, n_sp)
+    def _(d):
+        @pl.when((s < n_sp - 1) & (s - d >= 0))
+        def _():
+            send(kv_own, s, kup, d, s + 1).wait_send()
+
+        @pl.when((s > 0) & (s + d < n_sp))
+        def _():
+            send(kv_own, s, kdown, d, s - 1).wait_send()
+
+
 def layer_kernel(
-    n_sp, n_local, resid, hs, hl, gain, wts, wos, wol, wg_h, wu_h, wd_h, sg_h, su_h, sd_h,
+    n_sp, n_local, small, large, resid, heads_in, v_large, turn_c, turn_s, gain, wts, wos_h, wol_h, wg_h, wu_h, wd_h, sg_h, su_h, sd_h,
     out_ref,
-    wg, wu, wd, sg, su, sd, part, pc, psx, px, blk, stream, gath, acc, ybuf, rc, sx, rx, sz, rz, own,
-    wsem, psend, precv, zsend, xsend, csend, grecv, ycs, ycr, yxs, yxr, yzs, yzr,
+    wos, wol, wg, wu, wd, sg, su, sd, kv_own, kv, q_s, q_l, p_s, p_l, hs, hl, part, pc, psx, px, blk, stream, gath, acc, ybuf, rc, sx, rx, sz, rz, own,
+    wsem, kvr, kup, kdown, psend, precv, zsend, xsend, csend, grecv, ycs, ycr, yxs, yxr, yzs, yzr,
 ):
     s = lax.axis_index("sp")
     t = lax.axis_index("tp")
@@ -267,7 +360,7 @@
     loads = [
         pltpu.make_async_copy(src, dst, wsem.at[i])
         for i, (src, dst) in enumerate(
-            ((sg_h, sg), (su_h, su), (sd_h, sd), (wg_h, wg), (wu_h, wu), (wd_h, wd))
+            ((wos_h, wos), (wol_h, wol), (sg_h, sg), (su_h, su), (sd_h, sd), (wg_h, wg), (wu_h, wu), (wd_h, wd))
         )
     ]
     greet(peers)
@@ -277,6 +370,12 @@
     def strip(index):
         return pl.ds(pl.multiple_of(index * rows, rows), rows)
 
+    attention(
+        s, n_sp, small, large, heads_in, v_large, turn_c, turn_s,
+        kv_own, kv, q_s, q_l, p_s, p_l, hs, hl, kvr, kup, kdown,
+    )
+    loads[0].wait()
+    loads[1].wait()
     part[...] = (f32dot(hs[...], wos[...]) + f32dot(hl[...], wol[...])).astype(jnp.bfloat16)
     to_x = remote(part.at[strip(cxp)], pc.at[1], psend.at[0], precv.at[0], {"tp": cp})
     to_own = remote(part.at[strip(cp)], pc.at[0], psend.at[1], precv.at[1], {"tp": cp})
@@ -308,7 +407,7 @@
         copy.start()
     c_own.start()
     gath[s, strip(t)] = blk[...]
-    for load in loads:
+    for load in loads[2:]:
         load.wait()
 
     def block_of(k, column):
@@ -419,17 +518,26 @@
         x_part(k).wait_send()
 
 
-def layer_call(resid, hs, hl, gain, wts, wos, wol, wg, wu, wd, sg, su, sd):
+def layer_call(small, large, resid, heads_in, v_large, turn_c, turn_s, gain, wts, wos, wol, wg, wu, wd, sg, su, sd):
     n_sp = lax.axis_size("sp")
     n_tp = lax.axis_size("tp")
     rows, width = resid.shape
     n_local = wg.shape[0]
+    block = n_tp * rows
     padded = width + wts.shape[1]
     bf, f32 = jnp.bfloat16, jnp.float32
     dma = pltpu.SemaphoreType.DMA
     vmem = pl.BlockSpec(memory_space=pltpu.VMEM)
     anywhere = pl.BlockSpec(memory_space=pl.ANY)
-    scratch = [pltpu.VMEM(w.shape, w.dtype) for w in (wg, wu, wd, sg, su, sd)] + [
+    scratch = [pltpu.VMEM(w.shape, w.dtype) for w in (wos, wol, wg, wu, wd, sg, su, sd)] + [
+        pltpu.VMEM((block, 384), bf),
+        pltpu.VMEM((n_sp, block, 384), bf),
+        pltpu.VMEM((wos.shape[0] // small * block, small), bf),
+        pltpu.VMEM((wol.shape[0] // large * block, large), bf),
+        pltpu.VMEM((wos.shape[0] // small * block, n_sp * block), f32),
+        pltpu.VMEM((wol.shape[0] // large * block, n_sp * block), f32),
+        pltpu.VMEM((block, wos.shape[0]), bf),
+        pltpu.VMEM((block, wol.shape[0]), bf),
         pltpu.VMEM((n_tp * rows, width), bf),
         pltpu.VMEM((2, rows, width), bf),
         pltpu.VMEM((rows, width), bf),
@@ -445,34 +553,36 @@
         pltpu.VMEM((n_sp, rows, width), bf),
         pltpu.VMEM((n_sp, rows, width), bf),
         pltpu.VMEM((rows, width), f32),
-        dma((6,)), dma((3,)), dma((3,)),
+        dma((8,)), dma((n_sp,)), dma((n_sp,)), dma((n_sp,)), dma((3,)), dma((3,)),
         dma((n_sp - 1,)), dma((n_sp,)), dma((n_sp, 2)), dma((n_sp, n_tp)),
         dma((n_sp, 2)), dma((n_sp, 2)), dma((n_sp,)), dma((n_sp,)), dma((n_sp,)), dma((n_sp,)),
     ]
     return pl.pallas_call(
-        functools.partial(layer_kernel, n_sp, n_local),
+        functools.partial(layer_kernel, n_sp, n_local, small, large),
         out_shape=jax.ShapeDtypeStruct((rows, width), bf),
-        in_specs=[vmem] * 7 + [anywhere] * 6,
+        in_specs=[vmem] * 7 + [anywhere] * 8,
         out_specs=vmem,
         scratch_shapes=scratch,
         compiler_params=pltpu.CompilerParams(
-            collective_id=2, has_side_effects=True, vmem_limit_bytes=48 * 1024 * 1024
+            collective_id=2, has_side_effects=True, vmem_limit_bytes=58 * 1024 * 1024
         ),
-    )(resid, hs, hl, gain, wts, wos, wol, wg, wu, wd, sg, su, sd)
-
-
-def attend(queries, keys, values):
-    rows, heads, group, channels = queries.shape
-    keys = keys.reshape(keys.shape[0], heads, channels)
-    values = values.reshape(values.shape[0], heads, channels)
-    scores = jnp.einsum("qkgd,skd->kgqs", queries, keys, preferred_element_type=jnp.float32) * channels ** (-0.5)
-    raised = jnp.exp(scores - jnp.max(scores, axis=-1, keepdims=True))
-    totals = jnp.sum(raised, axis=-1)
-    mixture = jnp.einsum(
-        "kgqs,skd->qkgd", raised.astype(jnp.bfloat16), values, preferred_element_type=jnp.float32
-    )
-    mixture = mixture / jnp.transpose(totals, (2, 0, 1))[..., None]
-    return mixture.reshape(rows, -1).astype(jnp.bfloat16)
+    )(resid, heads_in, v_large, turn_c, turn_s, gain, wts, wos, wol, wg, wu, wd, sg, su, sd)
+
+
+def turn_table(positions, gain, width):
+    channels = gain.shape[0]
+    quarter, half = channels // 4, channels // 2
+    inverse = 1.0 / rope_base ** (jnp.arange(quarter, dtype=jnp.float32) / quarter)
+    by_row = (positions // GRID_W).astype(jnp.float32)[:, None] * inverse[None, :]
+    by_column = (positions % GRID_W).astype(jnp.float32)[:, None] * inverse[None, :]
+    angles = jnp.concatenate([by_row, by_row, by_column, by_column], axis=1)
+    parted = gain.reshape(2, 2, quarter)
+    facing = jnp.stack([-parted[:, 1], parted[:, 0]], axis=1).reshape(channels)
+    copies = width // channels
+    return (
+        jnp.tile(jnp.cos(angles) * gain, (1, copies)),
+        jnp.tile(jnp.sin(angles) * facing, (1, copies)),
+    )
 
 
 def dense_local(
@@ -482,20 +592,16 @@
 ):
     local_rows = q_small.shape[0]
     positions = lax.axis_index("sp") * local_rows + jnp.arange(local_rows, dtype=jnp.int32)
-    key_small = norm_rotate(k_small, gain_ks, positions, GRID_W)
-    key_large = norm_rotate(k_large, gain_kl, positions, GRID_W)
-    kv_small, kv_large = key_small.shape[1], key_large.shape[1]
-    pack = jnp.concatenate(
-        [key_small.reshape(local_rows, -1), v_small, key_large.reshape(local_rows, -1), v_large], axis=1
-    )
-    gathered = gather_rows(pack)
-    query_small = norm_rotate(q_small, gain_qs, positions, GRID_W)
-    query_large = norm_rotate(q_large, gain_ql, positions, GRID_W)
-    query_small = query_small.reshape(local_rows, kv_small, -1, gain_qs.shape[0])
-    query_large = query_large.reshape(local_rows, kv_large, -1, gain_ql.shape[0])
-    a, b = k_small.shape[1], k_large.shape[1]
-    heads_small = attend(query_small, gathered[:, :a], gathered[:, a : 2 * a])
-    heads_large = attend(query_large, gathered[:, 2 * a : 2 * a + b], gathered[:, 2 * a + b :])
+    small, large = gain_qs.shape[0], gain_ql.shape[0]
+    turns = [
+        turn_table(positions, gain, width)
+        for gain, width in (
+            (gain_qs, q_small.shape[1]), (gain_ks, 128), (gain_ql, q_large.shape[1]), (gain_kl, large),
+        )
+    ]
+    turn_c = jnp.concatenate([c for c, _ in turns], axis=1)
+    turn_s = jnp.concatenate([v for _, v in turns], axis=1)
+    heads_in = jnp.concatenate([q_small, k_small, v_small, q_large, k_large], axis=1)
     experts = w_gate.shape[0] * lax.axis_size("sp")
     named = routes[:, :, None] == jnp.arange(experts, dtype=jnp.int32)
     marks = jnp.sum(jnp.where(named, route_w[:, :, None], 0.0), axis=1)
@@ -505,13 +611,18 @@
     marks = jnp.concatenate([first, second, third], axis=1)
     marks = jnp.pad(marks, ((0, 0), (0, 128 - marks.shape[1]))).astype(jnp.bfloat16)
     return layer_call(
-        residual_in, heads_small, heads_large, g_ffn[None, :], marks, w_out_small, w_out_large,
+        small, large, residual_in, heads_in, v_large, turn_c, turn_s, g_ffn[None, :], marks, w_out_small, w_out_large,
         w_gate, w_up, w_down, ws_gate, ws_up, ws_down,
     )
 
 
 def fits_dense(mesh, *arrays):
     routes, w_gate = arrays[14], arrays[16]
+    tp = mesh.shape["tp"]
+    if (arrays[7].shape[0], arrays[9].shape[0]) != (64, 128):
+        return False
+    if (arrays[2].shape[1], arrays[5].shape[1]) != (64 * tp, 128 * tp):
+        return False
     ways = mesh.shape["sp"] * mesh.shape["tp"]
     rows_dev = routes.shape[0] // (ways * mesh.shape["grp"])
     experts = w_gate.shape[0]

time: 128 us -> 115 us (0.90)
  Pallas kernels: 108 us -> 102 us
  matrix products: 4.79 us -> 0 us
  other arithmetic: 7.11 us -> 4.95 us
    pallas_call x2 -> x1, Pallas kernels: 108 us -> 102 us  [layer_call(): pl.pallas_call(functools.partial(layer_kernel, n_sp, n_local, small, larg...]
    dot_general x4 -> x0, matrix products: 4.79 us -> none  [the longest x2 2.55 us: attend(): jnp.einsum('kgqs,skd->qkgd', raised.astype(jnp.bfloat16), values, preferr...]
    unnamed x36 -> x23, local copies, waits for them, and re-layouts: 5.67 us -> 1.99 us
    reshape x2 -> x4, local copies, waits for them, and re-layouts: 1.14 us -> 2.95 us  [turn_table(): parted = gain.reshape(2, 2, quarter)]
    reduce_sum x6 -> x0, other arithmetic: 1.37 us -> none  [the longest x2 1.06 us: attend(): totals = jnp.sum(raised, axis=-1)]
    mul x4 -> x6, other arithmetic: 1.73 us -> 2.89 us  [the longest x2 2.03 us: turn_table(): jnp.sin(angles) * facing]
where the time goes in v2:
time: 115 us
  Pallas kernels  102 us (89%)
  local copies, waits for them, and re-layouts  7.55 us (7%)
  other arithmetic  4.95 us (4%)
    pallas_call x1, Pallas kernels, layer_call(): pl.pallas_call(functools.partial(layer_kernel, n_sp, n_local, small, larg...  102 us
    reshape x4, local copies, waits for them, and re-layouts, turn_table(): parted = gain.reshape(2, 2, quarter)  2.95 us

profile of v2, /device:TPU:0, one launch (start us, length us, event | category | flops | bytes accessed | tf_op | source)
XLA Modules:
  0.0 114.8 jit_solution(6410417576249883827)
XLA Ops:
  0.0 0.1 broadcast_multiply_fusion.5
  0.2 0.7 reshape.417
  0.9 0.1 mul.224
  1.0 0.7 reshape.418
  1.8 0.1 mul.227
  1.9 1.2 %broadcast_multiply_fusion.1 = (f32[256,128]{1,0:T(8,128)S(1)}, f32[256,128]{1,0:T(8,128)S(1)}, f32[256,128]{1,0:T(8,128)S(1)}) fusion(f32[128]{0:T(128)S(1)} %mul.224, f32[256,32]{1,0:T(8,128)S(1)} %get-tuple-element.25, f32[256,32]{1,0:T(8,128)S(1)} %get-tuple-element.24, f32[128]{0:T(128)S(1)} %mul.227, f32[128]{0:T(128)} %param.32), kind=kLoop, calls=%fused_computation.7 | loop fusion | flops 196608 | bytes 460288 | tf_op jit(solution)/shard_map/mul | solution.py:584
  3.1 0.1 tile.64
  3.2 0.0 copy-start.5
  3.2 0.1 broadcast_multiply_fusion.7
  3.3 0.7 reshape.415
  4.1 0.1 mul.218
  4.2 0.7 reshape.416
  4.9 0.1 mul.221
  5.0 0.8 fusion.5
  5.8 0.0 copy-start.6
  5.9 0.1 copy.48
  6.0 0.1 copy.49
  6.1 1.0 pad_maximum_fusion.1.turn_s
  7.1 0.0 copy-start.7
  7.1 0.0 copy-start.8
  7.1 0.0 copy-start.3
  7.1 0.0 copy-start.4
  7.1 0.1 copy.47
  7.2 0.0 copy-done.5
  7.2 0.0 copy-start
  7.3 0.0 copy-start.1
  7.3 0.0 copy-start.2
  7.3 0.5 broadcast_multiply_fusion.3
  7.8 0.1 tile.28
  7.9 0.0 copy-done.6
  8.0 0.1 fusion.3
  8.1 0.1 copy.46
  8.2 1.0 pad_maximum_fusion.turn_c
  9.2 0.0 copy-done.7
  9.2 0.0 copy-done.8
  9.2 0.1 copy.50
  9.3 0.6 pad.5.wts
  10.0 0.0 copy-done.3
  10.0 0.1 copy.44
  10.1 0.0 copy-done.4
  10.1 0.1 copy.45
  10.2 0.0 copy-done
  10.2 0.0 copy-done.1
  10.2 0.0 copy-done.2
  10.2 0.9 concatenate.43.heads_in
  11.1 102.0 %shard_map.208 = bf16[64,2048]{1,0:T(8,128)(2,1)} custom-call(bf16[64,2048]{1,0:T(8,128)(2,1)} %resid.1, bf16[256,768]{1,0:T(8,128)(2,1)} %concatenate.43.heads_in, bf16[256,128]{1,0:T(8,128)(2,1)} %v_large.1, f32[256,768]{1,0:T(8,128)} %pad_maximum_fusion.turn_c, f32[256,768]{1,0:T(8,128)} %pad_maximum_fusion.1.turn_s, f32[1,2048]{1,0:T(1,128)} %bitcast.21, ...), custom_call_target="tpu_custom_call" | custom-call | tf_op jit(solution)/shard_map/pallas_call | solution.py:560
  113.1 1.7 %copy.58 = bf16[64,2048]{1,0:T(8,128)(2,1)} copy(bf16[64,2048]{1,0:T(8,128)(2,1)} %shard_map.208) | data formatting | bytes 524288
  (20 shorter events, 0.2 us)
Async XLA Ops:
  3.2 4.1 %copy-start.5 = (f32[128]{0:T(128)S(1)}, f32[128]{0:T(128)}, u32[]{:S(2)}) copy-start(f32[128]{0:T(128)} %param.31) | copy-start | bytes 1540
  5.8 2.1 %copy-start.6 = (f32[64]{0:T(128)S(1)}, f32[64]{0:T(128)}, u32[]{:S(2)}) copy-start(f32[64]{0:T(128)} %param.29) | copy-start | bytes 772
  7.1 2.1 %copy-start.7 = (f32[64,4]{0,1:T(4,128)S(1)}, f32[64,4]{0,1:T(4,128)}, u32[]{:S(2)}) copy-start(f32[64,4]{0,1:T(4,128)} %param.37) | copy-start | bytes 3076
  7.1 2.1 %copy-start.8 = (s32[64,4]{0,1:T(4,128)S(1)}, s32[64,4]{0,1:T(4,128)}, u32[]{:S(2)}) copy-start(s32[64,4]{0,1:T(4,128)} %param.36) | copy-start | bytes 3076
  7.1 2.8 %copy-start.3 = (bf16[256,64]{0,1:T(8,128)(2,1)S(1)}, bf16[256,64]{0,1:T(8,128)(2,1)}, u32[]{:S(2)}) copy-start(bf16[256,64]{0,1:T(8,128)(2,1)} %param.24) | copy-start | bytes 98308
  7.1 3.0 %copy-start.4 = (bf16[256,64]{0,1:T(8,128)(2,1)S(1)}, bf16[256,64]{0,1:T(8,128)(2,1)}, u32[]{:S(2)}) copy-start(bf16[256,64]{0,1:T(8,128)(2,1)} %param.25) | copy-start | bytes 98308
  7.2 3.0 %copy-start = (bf16[256,256]{1,0:T(8,128)(2,1)S(1)}, bf16[256,256]{1,0:T(8,128)(2,1)}, u32[]{:S(2)}) copy-start(bf16[256,256]{1,0:T(8,128)(2,1)} %param.23) | copy-start | bytes 393220
  7.3 3.0 %copy-start.1 = (bf16[256,256]{1,0:T(8,128)(2,1)S(1)}, bf16[256,256]{1,0:T(8,128)(2,1)}, u32[]{:S(2)}) copy-start(bf16[256,256]{1,0:T(8,128)(2,1)} %param.26) | copy-start | bytes 393220
  7.3 3.0 %copy-start.2 = (bf16[256,128]{1,0:T(8,128)(2,1)S(1)}, bf16[256,128]{1,0:T(8,128)(2,1)}, u32[]{:S(2)}) copy-start(bf16[256,128]{1,0:T(8,128)(2,1)} %param.27) | copy-start | bytes 196612

commit v3 on v2

--- a/solution.py
+++ b/solution.py
@@ -428,17 +428,24 @@
     def z_part(k):
         return remote(sz.at[k], rz.at[k], yzs.at[k], yzr.at[k], {"sp": lax.rem(s - k + n_sp, n_sp)})
 
+    def spread(k):
+        ahead = pass_on(k, t, xsend.at[k], {"tp": xp})
+        ahead.wait_recv()
+        ahead.start()
+        pass_on(k, t, csend.at[k, 0], {"tp": cp}).start()
+
+    if n_sp > 1:
+        spread(1)
+
     @pl.loop(0, n_sp + 2)
-    def _(k):
-        @pl.when(k < n_sp - 1)
-        def _():
-            ahead = pass_on(k + 1, t, xsend.at[k + 1], {"tp": xp})
-            ahead.wait_recv()
-            ahead.start()
-            pass_on(k + 1, t, csend.at[k + 1, 0], {"tp": cp}).start()
-
-        @pl.when(k < n_sp)
-        def _():
+    def _(step):
+        @pl.when(step < n_sp - 2)
+        def _():
+            spread(step + 2)
+
+        @pl.when(step < n_sp)
+        def _():
+            k = lax.rem(step + 1, n_sp)
             over = pass_on(k, xp, csend.at[k, 1], {"tp": cp})
             over.wait_recv()
             over.start()
@@ -471,16 +478,16 @@
             core_part(k, 1).start()
             core_part(k, 0).start()
 
-        @pl.when((k >= 1) & (k <= n_sp))
-        def _():
-            j = k - 1
+        @pl.when((step >= 1) & (step <= n_sp))
+        def _():
+            j = lax.rem(step, n_sp)
             core_part(j, 1).wait_recv()
             sx[j] = (ybuf[j, strip(xp)].astype(jnp.float32) + rc[j, 1].astype(jnp.float32)).astype(jnp.bfloat16)
             x_part(j).start()
 
-        @pl.when(k >= 2)
-        def _():
-            j = k - 2
+        @pl.when(step >= 2)
+        def _():
+            j = lax.rem(step - 1, n_sp)
             core_part(j, 0).wait_recv()
             x_part(j).wait_recv()
             total = ybuf[j, strip(t)].astype(jnp.float32) + rc[j, 0].astype(jnp.float32) + rx[j].astype(jnp.float32)

time: 115 us -> 111 us (0.965)
  Pallas kernels: 102 us -> 98.4 us
    pallas_call x1, Pallas kernels: 102 us -> 98.4 us  [layer_call(): pl.pallas_call(functools.partial(layer_kernel, n_sp, n_local, small, larg...]
where the time goes in v3:
time: 111 us
  Pallas kernels  98.4 us (89%)
  local copies, waits for them, and re-layouts  7.55 us (7%)
  other arithmetic  4.95 us (4%)
    pallas_call x1, Pallas kernels, layer_call(): pl.pallas_call(functools.partial(layer_kernel, n_sp, n_local, small, larg...  98.4 us
    reshape x4, local copies, waits for them, and re-layouts, turn_table(): parted = gain.reshape(2, 2, quarter)  2.95 us

profile of v3, /device:TPU:0, one launch (start us, length us, event | category | flops | bytes accessed | tf_op | source)
XLA Modules:
  0.0 111.2 jit_solution(3056912856099370750)
XLA Ops:
  0.0 0.1 broadcast_multiply_fusion.5
  0.2 0.7 reshape.417
  0.9 0.1 mul.224
  1.0 0.7 reshape.418
  1.8 0.1 mul.227
  1.9 1.2 %broadcast_multiply_fusion.1 = (f32[256,128]{1,0:T(8,128)S(1)}, f32[256,128]{1,0:T(8,128)S(1)}, f32[256,128]{1,0:T(8,128)S(1)}) fusion(f32[128]{0:T(128)S(1)} %mul.224, f32[256,32]{1,0:T(8,128)S(1)} %get-tuple-element.25, f32[256,32]{1,0:T(8,128)S(1)} %get-tuple-element.24, f32[128]{0:T(128)S(1)} %mul.227, f32[128]{0:T(128)} %param.32), kind=kLoop, calls=%fused_computation.7 | loop fusion | flops 196608 | bytes 460288 | tf_op jit(solution)/shard_map/mul | solution.py:591
  3.1 0.1 tile.64
  3.2 0.0 copy-start.5
  3.2 0.1 broadcast_multiply_fusion.7
  3.3 0.7 reshape.415
  4.1 0.1 mul.218
  4.2 0.7 reshape.416
  4.9 0.1 mul.221
  5.0 0.8 fusion.5
  5.8 0.0 copy-start.6
  5.9 0.1 copy.48
  6.0 0.1 copy.49
  6.1 1.0 pad_maximum_fusion.1.turn_s
  7.1 0.0 copy-start.7
  7.1 0.0 copy-start.8
  7.1 0.0 copy-start.3
  7.1 0.0 copy-start.4
  7.1 0.1 copy.47
  7.2 0.0 copy-done.5
  7.2 0.0 copy-start
  7.3 0.0 copy-start.1
  7.3 0.0 copy-start.2
  7.3 0.5 broadcast_multiply_fusion.3
  7.8 0.1 tile.28
  7.9 0.0 copy-done.6
  8.0 0.1 fusion.3
  8.1 0.1 copy.46
  8.2 1.0 pad_maximum_fusion.turn_c
  9.2 0.0 copy-done.7
  9.2 0.0 copy-done.8
  9.2 0.1 copy.50
  9.3 0.6 pad.5.wts
  10.0 0.0 copy-done.3
  10.0 0.1 copy.44
  10.1 0.0 copy-done.4
  10.1 0.1 copy.45
  10.2 0.0 copy-done
  10.2 0.0 copy-done.1
  10.2 0.0 copy-done.2
  10.2 0.9 concatenate.43.heads_in
  11.1 98.4 %shard_map.208 = bf16[64,2048]{1,0:T(8,128)(2,1)} custom-call(bf16[64,2048]{1,0:T(8,128)(2,1)} %resid.1, bf16[256,768]{1,0:T(8,128)(2,1)} %concatenate.43.heads_in, bf16[256,128]{1,0:T(8,128)(2,1)} %v_large.1, f32[256,768]{1,0:T(8,128)} %pad_maximum_fusion.turn_c, f32[256,768]{1,0:T(8,128)} %pad_maximum_fusion.1.turn_s, f32[1,2048]{1,0:T(1,128)} %bitcast.21, ...), custom_call_target="tpu_custom_call" | custom-call | tf_op jit(solution)/shard_map/pallas_call | solution.py:567
  109.5 1.7 %copy.58 = bf16[64,2048]{1,0:T(8,128)(2,1)} copy(bf16[64,2048]{1,0:T(8,128)(2,1)} %shard_map.208) | data formatting | bytes 524288
  (20 shorter events, 0.2 us)
Async XLA Ops:
  3.2 4.1 %copy-start.5 = (f32[128]{0:T(128)S(1)}, f32[128]{0:T(128)}, u32[]{:S(2)}) copy-start(f32[128]{0:T(128)} %param.31) | copy-start | bytes 1540
  5.8 2.1 %copy-start.6 = (f32[64]{0:T(128)S(1)}, f32[64]{0:T(128)}, u32[]{:S(2)}) copy-start(f32[64]{0:T(128)} %param.29) | copy-start | bytes 772
  7.1 2.1 %copy-start.7 = (f32[64,4]{0,1:T(4,128)S(1)}, f32[64,4]{0,1:T(4,128)}, u32[]{:S(2)}) copy-start(f32[64,4]{0,1:T(4,128)} %param.37) | copy-start | bytes 3076
  7.1 2.1 %copy-start.8 = (s32[64,4]{0,1:T(4,128)S(1)}, s32[64,4]{0,1:T(4,128)}, u32[]{:S(2)}) copy-start(s32[64,4]{0,1:T(4,128)} %param.36) | copy-start | bytes 3076
  7.1 2.8 %copy-start.3 = (bf16[256,64]{0,1:T(8,128)(2,1)S(1)}, bf16[256,64]{0,1:T(8,128)(2,1)}, u32[]{:S(2)}) copy-start(bf16[256,64]{0,1:T(8,128)(2,1)} %param.24) | copy-start | bytes 98308
  7.1 3.0 %copy-start.4 = (bf16[256,64]{0,1:T(8,128)(2,1)S(1)}, bf16[256,64]{0,1:T(8,128)(2,1)}, u32[]{:S(2)}) copy-start(bf16[256,64]{0,1:T(8,128)(2,1)} %param.25) | copy-start | bytes 98308
  7.2 3.0 %copy-start = (bf16[256,256]{1,0:T(8,128)(2,1)S(1)}, bf16[256,256]{1,0:T(8,128)(2,1)}, u32[]{:S(2)}) copy-start(bf16[256,256]{1,0:T(8,128)(2,1)} %param.23) | copy-start | bytes 393220
  7.3 3.0 %copy-start.1 = (bf16[256,256]{1,0:T(8,128)(2,1)S(1)}, bf16[256,256]{1,0:T(8,128)(2,1)}, u32[]{:S(2)}) copy-start(bf16[256,256]{1,0:T(8,128)(2,1)} %param.26) | copy-start | bytes 393220
  7.3 3.0 %copy-start.2 = (bf16[256,128]{1,0:T(8,128)(2,1)S(1)}, bf16[256,128]{1,0:T(8,128)(2,1)}, u32[]{:S(2)}) copy-start(bf16[256,128]{1,0:T(8,128)(2,1)} %param.27) | copy-start | bytes 196612
